TPU v7x, 32 devices: a whole 2x2x4 slice. The times are simulated.
32 devices in a mesh: fs: 16 (over z, y, x), tp: 2 (over core).
Axes of the slice: x: 2, y: 2, z: 4, core: 2. Of those that a mesh axis runs over, the one named last changes fastest.
Arguments:
- saved_inputs: bfloat16 [2048, 4096], P('fs', 'tp'), may hold values from -6 to 6
- value_cotangent: bfloat16 [2048, 2048], P('fs'), may hold values from -0.1875 to 0.1875
- glu_output: bfloat16 [2048, 2048], P('fs', 'tp'), may hold values from -6 to 6
- conv_cotangent: bfloat16 [2048, 2048], P('fs', 'tp'), may hold values from -0.125 to 0.125
- factor: bfloat16 [4096, 256], P('tp'), may hold values from -0.09375 to 0.09375
- value_weight: float32 [2048, 4096], P('fs', 'tp'), may hold values from -3 to 3
- first_moment: float32 [2048, 256], P('fs', 'tp'), may hold values from -6 to 6
- second_moment: float32 [2048, 256], P('fs', 'tp'), may hold values from 0.25 to 4
- kernel: float32 [31, 2048], P(None, 'tp'), may hold values from -1 to 1
- kernel_first: float32 [31, 2048], P(None, 'tp'), may hold values from -6 to 6
- kernel_second: float32 [31, 2048], P(None, 'tp'), may hold values from 0.25 to 4
Outputs:
- new_value: float32 [2048, 4096], P('fs', 'tp')
- value_copy: bfloat16 [2048, 4096], P('fs', 'tp')
- value_step: float32 [2048, 4096], P('fs', 'tp')
- new_first: float32 [2048, 256], P('fs', 'tp')
- new_second: float32 [2048, 256], P('fs', 'tp')
- new_kernel: float32 [31, 2048], P(None, 'tp')
- new_kernel_first: float32 [31, 2048], P(None, 'tp')
- new_kernel_second: float32 [31, 2048], P(None, 'tp')
All inputs are finite; a program needn't handle non-finite values.
Results may differ from a plain program's by a relative error of at most 0.0055.
Values may be sent and summed in bfloat16 or wider, within the bound.
A program may use at most 64 MiB of HBM per device.

v0:
```python
import jax
import jax.numpy as jnp
from jax import lax
from jax.sharding import PartitionSpec as P

WIDTH = 4096


def from_behind(x, axis, by):
    peers = lax.axis_size(axis)
    pairs = [(i, i + by) for i in range(peers) if 0 <= i + by < peers]
    return lax.ppermute(x, axis, pairs)


def body(
    saved_inputs,
    value_cotangent,
    glu_output,
    conv_cotangent,
    factor,
    value_weight,
    first_moment,
    second_moment,
    kernel,
    kernel_first,
    kernel_second,
):
    highest = lax.Precision.HIGHEST
    factor_f = factor.astype(jnp.float32)
    partial_reduced = jnp.dot(saved_inputs, factor, preferred_element_type=jnp.float32)
    reduced = lax.psum_scatter(
        partial_reduced.astype(jnp.bfloat16), "tp", scatter_dimension=1, tiled=True
    ).astype(jnp.float32)
    upper_part = reduced.astype(jnp.bfloat16)
    lower_part = (reduced - upper_part.astype(jnp.float32)).astype(jnp.bfloat16)
    dims = (((0,), (0,)), ((), ()))
    upper_term = lax.dot_general(
        value_cotangent, upper_part, dims, preferred_element_type=jnp.float32
    )
    lower_term = lax.dot_general(
        value_cotangent, lower_part, dims, preferred_element_type=jnp.float32
    )
    projected = lax.psum_scatter(upper_term + lower_term, "fs", scatter_dimension=0, tiled=True)
    new_first = 0.8 * first_moment + 0.2 * projected
    new_second = 0.9 * second_moment + 0.1 * projected * projected
    direction = new_first / jnp.sqrt(new_second)
    full_direction = lax.all_gather(direction, "tp", axis=1, tiled=True)
    back_proj = jnp.dot(full_direction, factor_f.T, precision=highest)
    row_squares = lax.psum(jnp.sum(back_proj * back_proj, axis=1), "tp")
    value_step = back_proj / jnp.sqrt(row_squares / WIDTH + 0.01)[:, None]
    new_value = value_weight - 0.05 * value_step
    value_copy = new_value.astype(jnp.bfloat16)
    token_count = glu_output.shape[0]
    reach = kernel.shape[0] - 1
    halo_rows = from_behind(glu_output[token_count - reach :], "fs", 1)
    extended = jnp.concatenate([halo_rows, glu_output], axis=0).astype(jnp.float32)
    cotangent_f = conv_cotangent.astype(jnp.float32)
    pieces = []
    for offset in range(kernel.shape[0]):
        begin = reach - offset
        pieces.append(jnp.sum(extended[begin : begin + token_count] * cotangent_f, axis=0))
    local_grad = jnp.stack(pieces, axis=0)
    kernel_grad = lax.psum(local_grad, "fs")
    new_kernel_first = 0.8 * kernel_first + 0.2 * kernel_grad
    new_kernel_second = 0.9 * kernel_second + 0.1 * kernel_grad * kernel_grad
    new_kernel = kernel - 0.05 * new_kernel_first / jnp.sqrt(new_kernel_second)
    return (
        new_value,
        value_copy,
        value_step,
        new_first,
        new_second,
        new_kernel,
        new_kernel_first,
        new_kernel_second,
    )


def solution(mesh):
    placed = (
        P("fs", "tp"),
        P("fs", None),
        P("fs", "tp"),
        P("fs", "tp"),
        P("tp", None),
        P("fs", "tp"),
        P("fs", "tp"),
        P("fs", "tp"),
        P(None, "tp"),
        P(None, "tp"),
        P(None, "tp"),
    )
    return jax.shard_map(
        body,
        mesh=mesh,
        in_specs=placed,
        out_specs=(
            P("fs", "tp"),
            P("fs", "tp"),
            P("fs", "tp"),
            P("fs", "tp"),
            P("fs", "tp"),
            P(None, "tp"),
            P(None, "tp"),
            P(None, "tp"),
        ),
        check_vma=False,
    )
```

profile of v0, /device:TPU:0, one launch (start us, length us, event | category | flops | bytes accessed | tf_op | source)
XLA Modules:
  0.0 225.3 jit_solution(7543839092658024599)
XLA Ops:
  8.0 0.0 copy-start
  8.0 0.0 reduce-scatter.7.cloned.1.call-start
  8.1 0.9 slice.96
  9.0 4.9 %collective-permute-start = (bf16[30,1024]{1,0:T(8,128)(2,1)S(1)}, bf16[30,1024]{1,0:T(8,128)(2,1)S(1)}, u32[]{:S(2)}, u32[]{:S(2)}) collective-permute-start(bf16[30,1024]{1,0:T(8,128)(2,1)S(1)} %slice.96), channel_id=1, source_target_pairs={{0,2},{2,4},{4,6},{6,8},{8,10},{10,12},{12,14},{14,16},{16,18},{18... | collective-permute-start | bytes 184328 | tf_op jit(solution)/shard_map/ppermute | solution.py:12
  13.9 0.0 copy-done
  13.9 0.0 copy-start.4
  13.9 1.4 convolution_convert_fusion
  15.3 0.7 copy.27
  16.0 0.0 reduce-scatter.7.cloned.1.call-update
  16.1 0.0 copy-start.3
  16.1 0.0 all-reduce.2.cloned.1.call-start
  16.1 0.0 collective-permute-done
  16.1 0.0 copy-done.4
  16.1 0.1 maximum_convert_fusion
  16.2 0.8 copy-done.3
  17.0 1.1 fusion.31
  18.1 0.8 fusion.30
  18.9 0.0 copy-start.1
  18.9 2.7 %stack.127 = f32[31,1024]{1,0:T(8,128)} concatenate(f32[1,1024]{1,0:T(1,128)S(1)} %bitcast.75, f32[1,1024]{1,0:T(1,128)S(1)} %bitcast.46, f32[1,1024]{1,0:T(1,128)S(1)} %bitcast.47, f32[1,1024]{1,0:T(1,128)S(1)} %bitcast.48, f32[1,1024]{1,0:T(1,128)S(1)} %bitcast.49, f32[1,1024]{1,0:T(1,128)S(1)} %bitcast.50, f32[1,1024]{1,0:T(1,128)S(1)} %bitcast.51, f32[1,1024]{1,0:T(1,128)S(1)} %bitcast.52, ...), dimensions={0} | concatenate | bytes 253952 | tf_op jit(solution)/shard_map/stack | solution.py:62
  21.6 0.0 all-reduce.2.cloned.1.call-update
  21.6 0.0 reduce-scatter.5.cloned.1.call-start
  21.7 2.4 %reduce-scatter.7.cloned.1.call-done = bf16[128,128]{1,0:T(8,128)(2,1)} async-done(((bf16[256,128]{1,0:T(8,128)(2,1)}), bf16[128,128]{1,0:T(8,128)(2,1)}) %reduce-scatter.7.cloned.1.call-update) | async-done | bytes 32784
  24.1 0.0 copy-start.8
  24.1 0.9 copy.28
  25.0 0.0 copy-done.1
  25.0 0.0 copy-done.8
  25.0 0.3 fusion.34
  25.3 1.3 fusion
  26.6 0.0 copy-start.9
  26.6 0.0 reduce-scatter.5.cloned.1.call-update
  26.6 0.8 copy-done.9
  27.5 0.1 copy.24
  27.6 0.0 copy-done.10
  27.6 0.1 copy.23
  27.7 100.1 %all-reduce.2.cloned.1.call-done = f32[31,1024]{1,0:T(8,128)} async-done(((f32[31,1024]{1,0:T(8,128)}), f32[31,1024]{1,0:T(8,128)}) %all-reduce.2.cloned.1.call-update) | async-done | bytes 126992 | tf_op jit(solution)/shard_map/psum | solution.py:63
  127.7 0.0 copy-done.7
  127.7 0.0 copy-done.5
  127.7 0.0 copy-done.6
  127.7 1.7 multiply_subtract_fusion.1
  129.4 78.8 %reduce-scatter.5.cloned.1.call-done = f32[128,128]{0,1:T(8,128)} async-done(((f32[2048,128]{0,1:T(8,128)}), f32[128,128]{0,1:T(8,128)}) %reduce-scatter.5.cloned.1.call-update) | async-done | bytes 65552 | tf_op jit(solution)/shard_map/reduce_scatter | solution.py:43
  208.2 0.9 rsqrt_multiply_fusion
  209.1 1.9 all_gather.3
  211.0 1.1 multiply_reduce_fusion
  212.1 2.5 %psum.14 = f32[128]{0:T(128)S(1)} all-reduce(f32[128]{0:T(128)S(1)} %get-tuple-element.64), channel_id=1, replica_groups=mesh['fs'=16,'tp'=2] {'tp'}, use_global_device_ids=true, to_apply=%region_3.0 | all-reduce | flops 128 | bytes 1024 | tf_op jit(solution)/shard_map/psum | solution.py:49
  214.5 0.7 copy.25
  215.3 0.7 copy.26
  216.0 0.0 copy-done.2
  216.0 1.8 fusion.37
  (6 shorter events, 0.0 us)
Async XLA Ops:
  8.0 5.9 %copy-start = (bf16[2048,256]{1,0:T(8,128)(2,1)S(1)}, bf16[2048,256]{1,0:T(8,128)(2,1)}, u32[]{:S(2)}) copy-start(bf16[2048,256]{1,0:T(8,128)(2,1)} %param.15) | copy-start | bytes 3145732
  8.0 16.1 %reduce-scatter.7.cloned.1.call-start = ((), (), s32[]{:S(2)}) async-start(), calls=%async_computation.4 | async-start | bytes 98304
  9.0 7.1 %collective-permute-start = (bf16[30,1024]{1,0:T(8,128)(2,1)S(1)}, bf16[30,1024]{1,0:T(8,128)(2,1)S(1)}, u32[]{:S(2)}, u32[]{:S(2)}) collective-permute-start(bf16[30,1024]{1,0:T(8,128)(2,1)S(1)} %slice.96), channel_id=1, source_target_pairs={{0,2},{2,4},{4,6},{6,8},{8,10},{10,12},{12,14},{14,16},{16,18},{18... | collective-permute-start | bytes 184328 | tf_op jit(solution)/shard_map/ppermute | solution.py:12
  13.9 2.2 copy-start.4
  16.1 1.0 copy-start.3
  16.1 111.7 %all-reduce.2.cloned.1.call-start = ((), (), s32[]{:S(2)}) async-start(), calls=%async_computation.3 | async-start | bytes 262144 | tf_op jit(solution)/shard_map/psum | solution.py:63
  18.9 6.1 %copy-start.1 = (bf16[128,2048]{1,0:T(8,128)(2,1)S(1)}, bf16[128,2048]{1,0:T(8,128)(2,1)}, u32[]{:S(2)}) copy-start(bf16[128,2048]{1,0:T(8,128)(2,1)} %param.12) | copy-start | bytes 1572868
  21.6 186.6 %reduce-scatter.5.cloned.1.call-start = ((), (), s32[]{:S(2)}) async-start(), calls=%async_computation.2 | async-start | bytes 1114112 | tf_op jit(solution)/shard_map/reduce_scatter | solution.py:43
  24.1 1.0 copy-start.8
  26.6 0.8 copy-start.9
  26.6 0.9 copy-start.10
  26.6 101.1 %copy-start.7 = (f32[31,1024]{1,0:T(8,128)S(1)}, f32[31,1024]{1,0:T(8,128)}, u32[]{:S(2)}) copy-start(f32[31,1024]{1,0:T(8,128)} %param.21) | copy-start | bytes 380932
  27.5 100.3 %copy-start.5 = (f32[31,1024]{1,0:T(8,128)S(1)}, f32[31,1024]{1,0:T(8,128)}, u32[]{:S(2)}) copy-start(f32[31,1024]{1,0:T(8,128)} %param.19) | copy-start | bytes 380932
  27.5 100.3 %copy-start.6 = (f32[31,1024]{1,0:T(8,128)S(1)}, f32[31,1024]{1,0:T(8,128)}, u32[]{:S(2)}) copy-start(f32[31,1024]{1,0:T(8,128)} %param.20) | copy-start | bytes 380932
  211.0 5.0 %copy-start.2 = (f32[128,2048]{1,0:T(8,128)S(1)}, f32[128,2048]{1,0:T(8,128)}, u32[]{:S(2)}) copy-start(f32[128,2048]{1,0:T(8,128)} %param.16) | copy-start | bytes 3145732
Sparse Core Ops, SparseCore 0:
  16.2 7.8 reduce-scatter.6
Sparse Core Ops, SparseCore 1:
  22.6 105.1 all-reduce.1
  130.4 77.7 reduce-scatter.4
where the time goes:
time: 226 us; the launch traced here: 225 us
  waiting for transfers between devices  181 us (80%)
  between operations  15.6 us (7%)
  local copies, waits for them, and re-layouts  8.54 us (4%)
  other arithmetic  6.33 us (3%)
  starting transfers between devices  5 us (2%)
  blocking collectives  4.37 us (2%)
  matrix products  4.05 us (2%)
    psum x1, waiting for transfers between devices, body(): kernel_grad = lax.psum(local_grad, 'fs')  100 us
    reduce_scatter x1, waiting for transfers between devices, body(): lax.psum_scatter(upper_term + lower_term, 'fs', scatter_dimension=0, tile...  78.8 us
    unnamed x28, local copies, waits for them, and re-layouts  4.95 us
    ppermute x1, starting transfers between devices, from_behind(): return lax.ppermute(x, axis, pairs)  4.87 us
  transfers between devices with their start and end apart: 4, of which 3 were waited for; matrix products, arithmetic and copies ran while one was open for 5% of the time, Pallas kernels for 0%

commit v1 on v0

--- a/solution.py
+++ b/solution.py
@@ -60,7 +60,11 @@
         begin = reach - offset
         pieces.append(jnp.sum(extended[begin : begin + token_count] * cotangent_f, axis=0))
     local_grad = jnp.stack(pieces, axis=0)
-    kernel_grad = lax.psum(local_grad, "fs")
+    kernel_grad = local_grad
+    for hop in (1, 2, 4, 8):
+        kernel_grad = kernel_grad + lax.ppermute(
+            kernel_grad, "fs", [(dev, dev ^ hop) for dev in range(16)]
+        )
     new_kernel_first = 0.8 * kernel_first + 0.2 * kernel_grad
     new_kernel_second = 0.9 * kernel_second + 0.1 * kernel_grad * kernel_grad
     new_kernel = kernel - 0.05 * new_kernel_first / jnp.sqrt(new_kernel_second)

time: 226 us -> 121 us (0.54)
  waiting for transfers between devices: 181 us -> 70.4 us
  starting transfers between devices: 5 us -> 16.3 us
  local copies, waits for them, and re-layouts: 8.54 us -> 5.71 us
    psum x1 -> x0, waiting for transfers between devices: 100 us -> none  [body(): kernel_grad = lax.psum(local_grad, 'fs')]
    reduce_scatter x1, waiting for transfers between devices: 78.8 us -> 42.4 us  [body(): lax.psum_scatter(upper_term + lower_term, 'fs', scatter_dimension=0, tile...]
    ppermute x0 -> x4, waiting for transfers between devices: none -> 15.6 us  [body(): lax.ppermute(kernel_grad, 'fs', [(dev, dev ^ hop) for dev in range(16)])]
    ppermute x0 -> x4, starting transfers between devices: none -> 12.5 us  [body(): lax.ppermute(kernel_grad, 'fs', [(dev, dev ^ hop) for dev in range(16)])]
    unnamed x4 -> x3, waiting for transfers between devices: 2.46 us -> 10.5 us
    another operation x1, local copies, waits for them, and re-layouts: 2.66 us -> 0.24 us  [body(): local_grad = jnp.stack(pieces, axis=0)]
  transfers between devices with their start and end apart: 4 -> 7, of which waited for: 3 -> 7; matrix products, arithmetic and copies ran while one was open for 5% -> 3% of each run, Pallas kernels for 0% -> 0%
where the time goes in v1:
time: 121 us; the launch traced here: 120 us
  waiting for transfers between devices  70.4 us (58%)
  starting transfers between devices  16.3 us (13%)
  between operations  14.2 us (12%)
  local copies, waits for them, and re-layouts  5.71 us (5%)
  other arithmetic  5.49 us (5%)
  blocking collectives  4.37 us (4%)
  matrix products  4.06 us (3%)
    reduce_scatter x1, waiting for transfers between devices, body(): lax.psum_scatter(upper_term + lower_term, 'fs', scatter_dimension=0, tile...  42.4 us
    ppermute x4, waiting for transfers between devices, body(): lax.ppermute(kernel_grad, 'fs', [(dev, dev ^ hop) for dev in range(16)])  15.6 us
    ppermute x4, starting transfers between devices, body(): lax.ppermute(kernel_grad, 'fs', [(dev, dev ^ hop) for dev in range(16)])  12.5 us
    unnamed x3, waiting for transfers between devices  10.5 us
    unnamed x28, local copies, waits for them, and re-layouts  5.45 us
    ppermute x1, starting transfers between devices, from_behind(): return lax.ppermute(x, axis, pairs)  3.72 us
    psum x1, blocking collectives, body(): row_squares = lax.psum(jnp.sum(back_proj * back_proj, axis=1), 'tp')  2.47 us
  transfers between devices with their start and end apart: 7, of which 7 were waited for; matrix products, arithmetic and copies ran while one was open for 3% of the time, Pallas kernels for 0%

profile of v1, /device:TPU:0, one launch (start us, length us, event | category | flops | bytes accessed | tf_op | source)
XLA Modules:
  0.0 120.5 jit_solution(5931972066683388435)
XLA Ops:
  7.2 0.0 copy-start
  7.2 0.0 reduce-scatter.7.cloned.1.call-start
  7.2 1.2 copy-done
  8.4 1.4 %convolution_convert_fusion = bf16[128,256]{1,0:T(8,128)(2,1)S(1)} fusion(bf16[128,2048]{1,0:T(8,128)(2,1)} %param.11, bf16[2048,256]{1,0:T(8,128)(2,1)S(1)} %copy-done), kind=kOutput, calls=%fused_computation.33 | convolution fusion | flops 134250496 | bytes 1638400 | tf_op jit(solution)/shard_map/dot_general | solution.py:30
  9.8 0.7 copy.27
  10.5 0.0 reduce-scatter.7.cloned.1.call-update
  10.6 0.0 reduce-scatter.5.cloned.1.call-start
  10.6 10.4 %reduce-scatter.7.cloned.1.call-done = bf16[128,128]{1,0:T(8,128)(2,1)} async-done(((bf16[256,128]{1,0:T(8,128)(2,1)}), bf16[128,128]{1,0:T(8,128)(2,1)}) %reduce-scatter.7.cloned.1.call-update) | async-done | bytes 32784
  21.0 0.9 copy.28
  22.0 0.0 copy-done.1
  22.0 0.0 copy-done.5
  22.0 0.3 fusion.34
  22.3 1.3 %fusion = f32[2048,128]{0,1:T(8,128)} fusion(f32[128,2048]{1,0:T(8,128)S(1)} %fusion.34, bf16[128,2048]{1,0:T(8,128)(2,1)S(1)} %copy-done.1, bf16[128,128]{1,0:T(8,128)(2,1)S(1)} %copy.28), kind=kOutput, calls=%fused_computation.32 | convolution fusion | flops 67420160 | bytes 2654208 | tf_op jit(solution)/shard_map/dot_general | solution.py:40
  23.6 0.0 reduce-scatter.5.cloned.1.call-update
  23.6 0.9 copy-done.4
  24.6 0.0 copy-start.3
  24.6 3.7 %collective-permute-start = (bf16[30,1024]{1,0:T(8,128)(2,1)S(1)}, bf16[30,1024]{1,0:T(8,128)(2,1)S(1)}, u32[]{:S(2)}, u32[]{:S(2)}) collective-permute-start(bf16[30,1024]{1,0:T(8,128)(2,1)S(1)} %slice.96), channel_id=1, source_target_pairs={{0,2},{2,4},{4,6},{6,8},{8,10},{10,12},{12,14},{14,16},{16,18},{18... | collective-permute-start | bytes 184328 | tf_op jit(solution)/shard_map/ppermute | solution.py:12
  28.3 1.9 %collective-permute-done = bf16[30,1024]{1,0:T(8,128)(2,1)S(1)} collective-permute-done((bf16[30,1024]{1,0:T(8,128)(2,1)S(1)}, bf16[30,1024]{1,0:T(8,128)(2,1)S(1)}, u32[]{:S(2)}, u32[]{:S(2)}) %collective-permute-start) | collective-permute-done | bytes 61472 | tf_op jit(solution)/shard_map/ppermute | solution.py:12
  30.2 0.1 maximum_convert_fusion
  30.3 0.0 copy-done.3
  30.3 0.8 fusion.30
  31.1 1.1 fusion.31
  32.2 0.2 stack.127
  32.4 2.5 %collective-permute-start.1 = (f32[31,1024]{1,0:T(8,128)S(1)}, f32[31,1024]{1,0:T(8,128)S(1)}, u32[]{:S(2)}, u32[]{:S(2)}) collective-permute-start(f32[31,1024]{1,0:T(8,128)S(1)} %stack.127), channel_id=1, source_target_pairs={{0,2},{2,0},{4,6},{6,4},{8,10},{10,8},{12,14},{14,12},{16,18},{18,... | collective-permute-start | bytes 380936 | tf_op jit(solution)/shard_map/ppermute | solution.py:65
  34.9 4.6 %collective-permute-done.1 = f32[31,1024]{1,0:T(8,128)S(1)} collective-permute-done((f32[31,1024]{1,0:T(8,128)S(1)}, f32[31,1024]{1,0:T(8,128)S(1)}, u32[]{:S(2)}, u32[]{:S(2)}) %collective-permute-start.1) | collective-permute-done | bytes 127008 | tf_op jit(solution)/shard_map/ppermute | solution.py:65
  39.5 2.8 %collective-permute-start.2 = (f32[31,1024]{1,0:T(8,128)S(1)}, f32[31,1024]{1,0:T(8,128)S(1)}, u32[]{:S(2)}, u32[]{:S(2)}) collective-permute-start(f32[31,1024]{1,0:T(8,128)S(1)} %add.48), channel_id=1, source_target_pairs={{0,4},{2,6},{4,0},{6,2},{8,12},{10,14},{12,8},{14,10},{16,20},{18,... | collective-permute-start | bytes 380936 | tf_op jit(solution)/shard_map/ppermute | solution.py:65
  42.4 3.3 %collective-permute-done.2 = f32[31,1024]{1,0:T(8,128)S(1)} collective-permute-done((f32[31,1024]{1,0:T(8,128)S(1)}, f32[31,1024]{1,0:T(8,128)S(1)}, u32[]{:S(2)}, u32[]{:S(2)}) %collective-permute-start.2) | collective-permute-done | bytes 127008 | tf_op jit(solution)/shard_map/ppermute | solution.py:65
  45.7 0.0 copy-start.9
  45.7 3.3 %collective-permute-start.3 = (f32[31,1024]{1,0:T(8,128)S(1)}, f32[31,1024]{1,0:T(8,128)S(1)}, u32[]{:S(2)}, u32[]{:S(2)}) collective-permute-start(f32[31,1024]{1,0:T(8,128)S(1)} %add.49), channel_id=1, source_target_pairs={{0,8},{2,10},{4,12},{6,14},{8,0},{10,2},{12,4},{14,6},{16,24},{18,... | collective-permute-start | bytes 380936 | tf_op jit(solution)/shard_map/ppermute | solution.py:65
  49.1 3.3 %collective-permute-done.3 = f32[31,1024]{1,0:T(8,128)S(1)} collective-permute-done((f32[31,1024]{1,0:T(8,128)S(1)}, f32[31,1024]{1,0:T(8,128)S(1)}, u32[]{:S(2)}, u32[]{:S(2)}) %collective-permute-start.3) | collective-permute-done | bytes 127008 | tf_op jit(solution)/shard_map/ppermute | solution.py:65
  52.4 0.0 copy-start.6
  52.4 0.0 copy-start.7
  52.4 3.8 %collective-permute-start.4 = (f32[31,1024]{1,0:T(8,128)S(1)}, f32[31,1024]{1,0:T(8,128)S(1)}, u32[]{:S(2)}, u32[]{:S(2)}) collective-permute-start(f32[31,1024]{1,0:T(8,128)S(1)} %add.50), channel_id=1, source_target_pairs={{0,16},{2,18},{4,20},{6,22},{8,24},{10,26},{12,28},{14,30},{16,0},... | collective-permute-start | bytes 380936 | tf_op jit(solution)/shard_map/ppermute | solution.py:65
  56.2 0.0 copy-done.9
  56.2 0.1 copy.24
  56.3 0.0 copy-done.10
  56.3 0.1 copy.23
  56.4 4.4 %collective-permute-done.4 = f32[31,1024]{1,0:T(8,128)S(1)} collective-permute-done((f32[31,1024]{1,0:T(8,128)S(1)}, f32[31,1024]{1,0:T(8,128)S(1)}, u32[]{:S(2)}, u32[]{:S(2)}) %collective-permute-start.4) | collective-permute-done | bytes 127008 | tf_op jit(solution)/shard_map/ppermute | solution.py:65
  60.8 0.0 copy-done.6
  60.8 0.8 multiply_subtract_fusion.1
  61.6 42.4 %reduce-scatter.5.cloned.1.call-done = f32[128,128]{0,1:T(8,128)} async-done(((f32[2048,128]{0,1:T(8,128)}), f32[128,128]{0,1:T(8,128)}) %reduce-scatter.5.cloned.1.call-update) | async-done | bytes 65552 | tf_op jit(solution)/shard_map/reduce_scatter | solution.py:43
  104.0 0.9 rsqrt_multiply_fusion
  104.9 1.9 %all_gather.3 = f32[128,256]{0,1:T(8,128)S(1)} all-gather(f32[128,128]{0,1:T(8,128)S(1)} %get-tuple-element.61), channel_id=1, replica_groups=mesh['fs'=16,'tp'=2] {'tp'}, dimensions={1}, use_global_device_ids=true | all-gather | bytes 196608 | tf_op jit(solution)/shard_map/all_gather | solution.py:47
  106.8 1.1 multiply_reduce_fusion
  107.9 2.5 %psum.7 = f32[128]{0:T(128)S(1)} all-reduce(f32[128]{0:T(128)S(1)} %get-tuple-element.64), channel_id=1, replica_groups=mesh['fs'=16,'tp'=2] {'tp'}, use_global_device_ids=true, to_apply=%region_3.0 | all-reduce | flops 128 | bytes 1024 | tf_op jit(solution)/shard_map/psum | solution.py:49
  110.4 0.7 copy.25
  111.1 0.7 copy.26
  111.8 1.8 %fusion.37 = (bf16[128,2048]{1,0:T(8,128)(2,1)}, f32[128,2048]{1,0:T(8,128)}, f32[128,2048]{1,0:T(8,128)}) fusion(f32[128,2048]{1,0:T(8,128)S(1)} %copy-done.2, f32[128,2048]{1,0:T(8,128)S(1)} %get-tuple-element.65, f32[128]{0:T(128)S(1)} %add_sqrt_fusion), kind=kLoop, calls=%fused_computation.81 | loop fusion | flops 1048576 | bytes 4719104 | tf_op jit(solution)/shard_map/convert_element_type | solution.py:52
  (14 shorter events, 0.1 us)
Async XLA Ops:
  7.2 1.2 %copy-start = (bf16[2048,256]{1,0:T(8,128)(2,1)S(1)}, bf16[2048,256]{1,0:T(8,128)(2,1)}, u32[]{:S(2)}) copy-start(bf16[2048,256]{1,0:T(8,128)(2,1)} %param.15) | copy-start | bytes 3145732
  7.2 13.9 %reduce-scatter.7.cloned.1.call-start = ((), (), s32[]{:S(2)}) async-start(), calls=%async_computation.3 | async-start | bytes 98304
  8.4 13.6 %copy-start.1 = (bf16[128,2048]{1,0:T(8,128)(2,1)S(1)}, bf16[128,2048]{1,0:T(8,128)(2,1)}, u32[]{:S(2)}) copy-start(bf16[128,2048]{1,0:T(8,128)(2,1)} %param.12) | copy-start | bytes 1572868
  10.6 93.5 %reduce-scatter.5.cloned.1.call-start = ((), (), s32[]{:S(2)}) async-start(), calls=%async_computation.2 | async-start | bytes 1114112 | tf_op jit(solution)/shard_map/reduce_scatter | solution.py:43
  21.0 1.0 copy-start.5
  23.6 0.9 copy-start.4
  24.6 5.7 %copy-start.3 = (bf16[128,1024]{1,0:T(8,128)(2,1)S(1)}, bf16[128,1024]{1,0:T(8,128)(2,1)}, u32[]{:S(2)}) copy-start(bf16[128,1024]{1,0:T(8,128)(2,1)} %param.14) | copy-start | bytes 786436
  24.6 5.6 %collective-permute-start = (bf16[30,1024]{1,0:T(8,128)(2,1)S(1)}, bf16[30,1024]{1,0:T(8,128)(2,1)S(1)}, u32[]{:S(2)}, u32[]{:S(2)}) collective-permute-start(bf16[30,1024]{1,0:T(8,128)(2,1)S(1)} %slice.96), channel_id=1, source_target_pairs={{0,2},{2,4},{4,6},{6,8},{8,10},{10,12},{12,14},{14,16},{16,18},{18... | collective-permute-start | bytes 184328 | tf_op jit(solution)/shard_map/ppermute | solution.py:12
  32.4 7.1 %collective-permute-start.1 = (f32[31,1024]{1,0:T(8,128)S(1)}, f32[31,1024]{1,0:T(8,128)S(1)}, u32[]{:S(2)}, u32[]{:S(2)}) collective-permute-start(f32[31,1024]{1,0:T(8,128)S(1)} %stack.127), channel_id=1, source_target_pairs={{0,2},{2,0},{4,6},{6,4},{8,10},{10,8},{12,14},{14,12},{16,18},{18,... | collective-permute-start | bytes 380936 | tf_op jit(solution)/shard_map/ppermute | solution.py:65
  39.5 6.1 %collective-permute-start.2 = (f32[31,1024]{1,0:T(8,128)S(1)}, f32[31,1024]{1,0:T(8,128)S(1)}, u32[]{:S(2)}, u32[]{:S(2)}) collective-permute-start(f32[31,1024]{1,0:T(8,128)S(1)} %add.48), channel_id=1, source_target_pairs={{0,4},{2,6},{4,0},{6,2},{8,12},{10,14},{12,8},{14,10},{16,20},{18,... | collective-permute-start | bytes 380936 | tf_op jit(solution)/shard_map/ppermute | solution.py:65
  45.7 10.5 %copy-start.9 = (f32[128,128]{1,0:T(8,128)S(1)}, f32[128,128]{1,0:T(8,128)}, u32[]{:S(2)}) copy-start(f32[128,128]{1,0:T(8,128)} %param.18) | copy-start | bytes 196612
  45.7 6.6 %collective-permute-start.3 = (f32[31,1024]{1,0:T(8,128)S(1)}, f32[31,1024]{1,0:T(8,128)S(1)}, u32[]{:S(2)}, u32[]{:S(2)}) collective-permute-start(f32[31,1024]{1,0:T(8,128)S(1)} %add.49), channel_id=1, source_target_pairs={{0,8},{2,10},{4,12},{6,14},{8,0},{10,2},{12,4},{14,6},{16,24},{18,... | collective-permute-start | bytes 380936 | tf_op jit(solution)/shard_map/ppermute | solution.py:65
  52.4 3.9 %copy-start.10 = (f32[128,128]{1,0:T(8,128)S(1)}, f32[128,128]{1,0:T(8,128)}, u32[]{:S(2)}) copy-start(f32[128,128]{1,0:T(8,128)} %param.17) | copy-start | bytes 196612
  52.4 8.4 %copy-start.8 = (f32[31,1024]{1,0:T(8,128)S(1)}, f32[31,1024]{1,0:T(8,128)}, u32[]{:S(2)}) copy-start(f32[31,1024]{1,0:T(8,128)} %param.21) | copy-start | bytes 380932
  52.4 8.4 %copy-start.6 = (f32[31,1024]{1,0:T(8,128)S(1)}, f32[31,1024]{1,0:T(8,128)}, u32[]{:S(2)}) copy-start(f32[31,1024]{1,0:T(8,128)} %param.19) | copy-start | bytes 380932
  52.4 8.4 %copy-start.7 = (f32[31,1024]{1,0:T(8,128)S(1)}, f32[31,1024]{1,0:T(8,128)}, u32[]{:S(2)}) copy-start(f32[31,1024]{1,0:T(8,128)} %param.20) | copy-start | bytes 380932
  52.4 8.4 %collective-permute-start.4 = (f32[31,1024]{1,0:T(8,128)S(1)}, f32[31,1024]{1,0:T(8,128)S(1)}, u32[]{:S(2)}, u32[]{:S(2)}) collective-permute-start(f32[31,1024]{1,0:T(8,128)S(1)} %add.50), channel_id=1, source_target_pairs={{0,16},{2,18},{4,20},{6,22},{8,24},{10,26},{12,28},{14,30},{16,0},... | collective-permute-start | bytes 380936 | tf_op jit(solution)/shard_map/ppermute | solution.py:65
  106.8 5.0 %copy-start.2 = (f32[128,2048]{1,0:T(8,128)S(1)}, f32[128,2048]{1,0:T(8,128)}, u32[]{:S(2)}) copy-start(f32[128,2048]{1,0:T(8,128)} %param.16) | copy-start | bytes 3145732
Sparse Core Ops, SparseCore 0:
  10.8 10.2 reduce-scatter.6
  23.9 80.1 reduce-scatter.4
